TPU v7x, 256 devices: a 2x2x32 block of a 4x8x32 slice. The times are simulated.
256 devices in a mesh: grp: 4 (over y, x), ep: 64 (over z, core).
Axes of the slice: x: 2, y: 2, z: 32, core: 2. Of those that a mesh axis runs over, the one named last changes fastest.
The devices are a block of a 4x8x32 slice.
Arguments:
- tokens: bfloat16 [32768, 2048], P(('grp', 'ep')), parts along dimension 0, may hold values from -6 to 6
- routing: int32 [32768, 2], P(('grp', 'ep')), parts along dimension 0, may hold values from 0 to 15, all different within a row; in each aligned block of 128 rows (0 to 127, 128 to 255, ...) at most 20 rows name the same one
- gates: float32 [32768, 2], P(('grp', 'ep')), parts along dimension 0, may hold values from 0.2 to 1
- norm_gain: bfloat16 [2048], replicated, may hold values from 0.099609375 to 1.8984375
- w_gate: bfloat16 [64, 2048, 896], P('ep'), may hold values from -0.125 to 0.125
- w_up: bfloat16 [64, 2048, 896], P('ep'), may hold values from -0.125 to 0.125
- w_down: bfloat16 [64, 896, 2048], P('ep'), may hold values from -0.09375 to 0.09375
Outputs:
- mixed: bfloat16 [32768, 2048], P(('grp', 'ep')), parts along dimension 0
There are 4 independent parts, one for each index of `grp`. A program takes and returns all parts, laid end to end along the dimension named above; an argument that names none is the same for every part. Nothing has to cross between parts.
Inputs may be any that keep to these rules, and one draw needn't show every extreme that they name: `routing`: each row names 2 different experts. Among the rows of one device at most 20 name any one expert, and in every draw some expert is named by exactly 20 rows of some device.
All inputs are finite; a program needn't handle non-finite values.
Results may differ from a plain program's by a relative error of at most 0.0078.
Values may be sent and summed in bfloat16 or wider, within the bound.
A program may use at most 128 MiB of HBM per device.

v0:
```python
import jax
import jax.numpy as jnp
from jax import lax
from jax.sharding import PartitionSpec as P

GROUP = 4


def partner_2(x, axis, distance):
    return lax.ppermute(x, axis, [(i, i ^ 1 << distance) for i in range(lax.axis_size(axis))])


def per_device(tokens, routing, gates, norm_gain, w_gate, w_up, w_down):
    tok_count, model_width = tokens.shape
    top_count = routing.shape[1]
    devices = lax.axis_size("ep")
    experts = devices // GROUP
    member_slots = 5 * tok_count * top_count // (4 * devices)
    capacity = GROUP * member_slots
    group_bits = GROUP.bit_length() - 1
    own_index = lax.axis_index("ep")
    values = tokens.astype(jnp.float32)
    scale = lax.rsqrt(jnp.mean(values * values, axis=-1, keepdims=True) + 1e-06)
    normed = (values * scale * norm_gain.astype(jnp.float32)).astype(jnp.bfloat16)
    one_hot = (routing[..., None] == jnp.arange(experts, dtype=jnp.int32)).astype(jnp.int32)
    per_token = jnp.sum(one_hot, axis=1)
    before = jnp.cumsum(per_token, axis=0) - per_token
    slots = jnp.sum(one_hot * before[:, None, :], axis=-1)
    target = (routing * capacity + slots).reshape(-1)
    outgoing = jnp.zeros((experts * capacity, model_width), jnp.bfloat16)
    outgoing = outgoing.at[target].set(jnp.repeat(normed, top_count, axis=0))
    shares = lax.all_to_all(
        outgoing.reshape(devices, member_slots, model_width),
        "ep",
        split_axis=0,
        concat_axis=0,
        tiled=True,
    )
    pieces = shares[:, None]
    for bit_index in range(group_bits):
        partner = partner_2(pieces, "ep", bit_index)
        own_bit = own_index >> bit_index & 1
        lower_half = jnp.where(own_bit == 0, pieces, partner)
        upper_half = jnp.where(own_bit == 0, partner, pieces)
        pieces = jnp.concatenate([lower_half, upper_half], axis=1)
    arrived = pieces.reshape(devices, capacity, model_width)
    expert_rows = arrived.reshape(devices * capacity, model_width)
    gate_act = jnp.dot(expert_rows, w_gate[0], preferred_element_type=jnp.float32)
    up_act = jnp.dot(expert_rows, w_up[0], preferred_element_type=jnp.float32)
    hidden = (jax.nn.silu(gate_act) * up_act).astype(jnp.bfloat16)
    partial_value = jnp.dot(hidden, w_down[0], preferred_element_type=jnp.float32)
    summed = partial_value.reshape(devices, GROUP, member_slots, model_width)
    for bit_index in range(group_bits):
        halves = summed.reshape(devices, summed.shape[1] // 2, 2, member_slots, model_width)
        own_bit = own_index >> bit_index & 1
        kept_part = lax.dynamic_index_in_dim(halves, own_bit, 2, keepdims=False)
        given_part = lax.dynamic_index_in_dim(halves, 1 - own_bit, 2, keepdims=False)
        summed = kept_part + partner_2(given_part.astype(jnp.bfloat16), "ep", bit_index).astype(
            given_part.dtype
        )
    finished = summed.reshape(devices, member_slots, model_width).astype(jnp.bfloat16)
    returned = lax.all_to_all(finished, "ep", split_axis=0, concat_axis=0, tiled=True)
    picked = returned.reshape(experts * capacity, model_width)[target]
    picked = picked.reshape(tok_count, top_count, model_width)
    mixed = jnp.sum(gates[..., None] * picked.astype(jnp.float32), axis=1)
    return mixed.astype(jnp.bfloat16)


def solution(mesh):
    placed = (
        P(("grp", "ep"), None),
        P(("grp", "ep"), None),
        P(("grp", "ep"), None),
        P(),
        P("ep", None, None),
        P("ep", None, None),
        P("ep", None, None),
    )
    return jax.shard_map(
        per_device, mesh=mesh, in_specs=placed, out_specs=P(("grp", "ep"), None), check_vma=False
    )
```

profile of v0, /device:TPU:44, one launch (start us, length us, event | category | flops | bytes accessed | tf_op | source)
XLA Modules:
  0.0 638.1 jit_solution(1168048872367196716)
XLA Ops:
  3.4 1.2 fusion.8
  4.6 1.2 fusion.10
  6.9 2.5 scatter_custom_fusion
  9.5 1.6 reshape.76
  11.1 233.3 %all_to_all.10 = bf16[64,5,2048]{2,1,0:T(8,128)(2,1)S(1)} all-to-all(bf16[64,5,2048]{2,1,0:T(8,128)(2,1)} %reshape.76), channel_id=1, replica_groups=mesh['grp'=4,'ep'=64] {'ep'}, dimensions={0} | all-to-all | bytes 2621440 | tf_op jit(solution)/shard_map/all_to_all | solution.py:32
  244.4 0.9 copy.34
  245.4 3.1 collective-permute-done
  248.5 2.2 copy_select_fusion.3
  250.8 0.9 pad_maximum_fusion.1
  252.7 1.7 copy.37
  254.8 59.0 %collective-permute-done.1 = bf16[64,2,5,2048]{3,0,2,1:T(8,128)(2,1)} collective-permute-done((bf16[64,2,5,2048]{3,0,2,1:T(8,128)(2,1)S(1)}, bf16[64,2,5,2048]{3,0,2,1:T(8,128)(2,1)}, u32[]{:S(2)}, u32[]{:S(2)}) %collective-permute-start.1) | collective-permute-done | bytes 2621472 | tf_op jit(solution)/shard_map/ppermute | solution.py:10
  313.7 6.5 %copy_select_fusion.1 = (bf16[64,2,5,2048]{3,2,0,1:T(8,128)(2,1)}, bf16[64,2,5,2048]{3,2,0,1:T(8,128)(2,1)}) fusion(bf16[64,2,5,2048]{3,0,2,1:T(8,128)(2,1)} %collective-permute-done.1, pred[]{:T(512)S(6)} %eq.10, bf16[64,1,5,2048]{3,2,0,1:T(8,128)(2,1)} %copy-done.1, bf16[64,1,5,2048]{3,2,0,1:T(8,128)(2,1)} %copy-done), kind=kLoop, calls=%fused_computation.7 | loop fusion | flops 3932160 | bytes 10485761 | tf_op jit(solution)/shard_map/jit(_where)/select_n | solution.py:43
  320.3 8.4 %pad_maximum_fusion = bf16[64,4,5,2048]{3,2,0,1:T(8,128)(2,1)} fusion(bf16[64,2,5,2048]{3,2,0,1:T(8,128)(2,1)} %get-tuple-element.6, bf16[64,2,5,2048]{3,2,0,1:T(8,128)(2,1)} %get-tuple-element.5), kind=kLoop, calls=%fused_computation.2 | loop fusion | flops 2621440 | bytes 10485760 | tf_op jit(solution)/shard_map/concatenate | solution.py:45
  328.6 8.3 %copy.40 = bf16[64,4,5,2048]{3,2,1,0:T(8,128)(2,1)} copy(bf16[64,4,5,2048]{3,2,0,1:T(8,128)(2,1)} %pad_maximum_fusion) | data formatting | bytes 10485760 | tf_op jit(solution)/shard_map/concatenate | solution.py:45
  336.9 10.0 %reshape_reshape.4 = bf16[1280,2048]{1,0:T(8,128)(2,1)} reshape(bf16[64,4,5,2048]{3,2,1,0:T(8,128)(2,1)} %copy.40) | data formatting | bytes 10485760 | tf_op jit(solution)/shard_map/reshape;reshape | solution.py:47
  346.9 8.7 %fusion.3 = f32[1280,896]{1,0:T(8,128)S(1)} fusion(bf16[1280,2048]{1,0:T(8,128)(2,1)} %reshape_reshape.4, bf16[1,2048,896]{2,1,0:T(8,128)(2,1)} %param.11), kind=kOutput, calls=%fused_computation.12 | convolution fusion | flops 4697620480 | bytes 13500416 | tf_op jit(solution)/shard_map/dot_general | solution.py:48
  355.7 6.0 multiply_convert_fusion
  361.6 2.7 dot_general.13
  364.3 8.9 %fusion = f32[64,2,2,5,2048]{4,0,3,2,1:T(8,128)S(1)} fusion(bf16[1,896,2048]{2,1,0:T(8,128)(2,1)} %param.13, bf16[64,2,2,5,896]{4,3,2,1,0:T(8,128)(2,1)} %dot_general.13), kind=kOutput, calls=%fused_computation.9 | convolution fusion | flops 4697620480 | bytes 16449536 | tf_op jit(solution)/shard_map/dot_general | solution.py:51
  373.2 4.0 copy-done.3
  377.2 1.9 fusion.5
  379.1 5.1 collective-permute-done.2
  384.2 3.3 bitcast_add_fusion
  387.5 2.3 copy-done.2
  390.5 30.5 %collective-permute-done.3 = bf16[64,1,5,2048]{3,0,2,1:T(8,128)(2,1)S(1)} collective-permute-done((bf16[64,1,5,2048]{3,0,2,1:T(8,128)(2,1)S(1)}, bf16[64,1,5,2048]{3,0,2,1:T(8,128)(2,1)S(1)}, u32[]{:S(2)}, u32[]{:S(2)}) %collective-permute-start.3) | collective-permute-done | bytes 1310752 | tf_op jit(solution)/shard_map/ppermute | solution.py:10
  421.0 2.2 fusion.7
  423.2 2.1 copy.42
  425.3 6.8 %all-to-all-start.1 = ((bf16[64,5,2048]{2,1,0:T(8,128)(2,1)}), bf16[64,5,2048]{2,1,0:T(8,128)(2,1)S(1)}, u32[]{:S(2)}, u32[]{:S(2)}) async-start(bf16[64,5,2048]{2,1,0:T(8,128)(2,1)} %copy.42), calls=%async_computation.1 | async-start | bytes 4194304 | tf_op jit(solution)/shard_map/all_to_all | solution.py:62
  432.2 198.7 %all-to-all-done.1 = bf16[64,5,2048]{2,1,0:T(8,128)(2,1)S(1)} async-done(((bf16[64,5,2048]{2,1,0:T(8,128)(2,1)}), bf16[64,5,2048]{2,1,0:T(8,128)(2,1)S(1)}, u32[]{:S(2)}, u32[]{:S(2)}) %all-to-all-start.1) | async-done | bytes 1310752 | tf_op jit(solution)/shard_map/all_to_all | solution.py:62
  631.5 1.4 gather_fusion
  632.8 1.3 reshape.78
  634.2 3.9 multiply_reduce_fusion
  (34 shorter events, 7.2 us)
Async XLA Ops:
  245.2 3.3 collective-permute-start
  250.7 1.4 copy-start
  250.7 2.0 copy-start.1
  254.4 59.3 %collective-permute-start.1 = (bf16[64,2,5,2048]{3,0,2,1:T(8,128)(2,1)S(1)}, bf16[64,2,5,2048]{3,0,2,1:T(8,128)(2,1)}, u32[]{:S(2)}, u32[]{:S(2)}) collective-permute-start(bf16[64,2,5,2048]{3,0,2,1:T(8,128)(2,1)S(1)} %copy.37), channel_id=1, source_target_pairs={{0,2},{1,3},{2,0},{3,1},{4,6},{5,7},{6,4},{7,5},{8,10},{9,11},{10,... | collective-permute-start | bytes 7864328 | tf_op jit(solution)/shard_map/ppermute | solution.py:10
  346.9 8.7 %copy-start.4 = (bf16[1280,2048]{1,0:T(8,128)(2,1)S(1)}, bf16[1280,2048]{1,0:T(8,128)(2,1)}, u32[]{:S(2)}) copy-start(bf16[1280,2048]{1,0:T(8,128)(2,1)} %reshape_reshape.4) | copy-start | bytes 15728644
  346.9 8.8 %copy-start.6 = (bf16[1,2048,896]{2,1,0:T(8,128)(2,1)S(1)}, bf16[1,2048,896]{2,1,0:T(8,128)(2,1)}, u32[]{:S(2)}) copy-start(bf16[1,2048,896]{2,1,0:T(8,128)(2,1)} %param.12) | copy-start | bytes 11010052
  373.2 4.0 copy-start.3
  379.1 5.1 collective-permute-start.2
  387.5 2.3 copy-start.2
  390.0 30.9 %collective-permute-start.3 = (bf16[64,1,5,2048]{3,0,2,1:T(8,128)(2,1)S(1)}, bf16[64,1,5,2048]{3,0,2,1:T(8,128)(2,1)S(1)}, u32[]{:S(2)}, u32[]{:S(2)}) collective-permute-start(bf16[64,1,5,2048]{3,0,2,1:T(8,128)(2,1)S(1)} %dynamic-slice_convert_fusion.1), channel_id=1, source_target_pairs={{0,2},{1,3},{2,0},{3,1},{4,6},{5,7},{6,4},{7,5},{8,10},{9,11},{10,... | collective-permute-start | bytes 3932168 | tf_op jit(solution)/shard_map/ppermute | solution.py:10
  423.2 8.9 %copy-start.5 = (f32[128,2]{0,1:T(2,128)S(1)}, f32[128,2]{0,1:T(2,128)}, u32[]{:S(2)}) copy-start(f32[128,2]{0,1:T(2,128)} %param.9) | copy-start | bytes 3076
  425.3 205.6 %all-to-all-start.1 = ((bf16[64,5,2048]{2,1,0:T(8,128)(2,1)}), bf16[64,5,2048]{2,1,0:T(8,128)(2,1)S(1)}, u32[]{:S(2)}, u32[]{:S(2)}) async-start(bf16[64,5,2048]{2,1,0:T(8,128)(2,1)} %copy.42), calls=%async_computation.1 | async-start | bytes 4194304 | tf_op jit(solution)/shard_map/all_to_all | solution.py:62
where the time goes:
time: 639 us; the launch traced here: 638 us
  waiting for transfers between devices  296 us (46%)
  blocking collectives  233 us (36%)
  local copies, waits for them, and re-layouts  44 us (7%)
  other arithmetic  32.9 us (5%)
  matrix products  23.6 us (4%)
  starting transfers between devices  7.7 us (1%)
    all_to_all x1, blocking collectives, per_device(): lax.all_to_all(outgoing.reshape(devices, member_slots, model_width), 'ep'...  233 us
    all_to_all x1, waiting for transfers between devices, per_device(): lax.all_to_all(finished, 'ep', split_axis=0, concat_axis=0, tiled=True)  199 us
    ppermute x4, waiting for transfers between devices, partner_2(): lax.ppermute(x, axis, [(i, i ^ 1 << distance) for i in range(lax.axis_siz...  97.7 us
  transfers between devices with their start and end apart: 5, of which 5 were waited for; matrix products, arithmetic and copies ran while one was open for 0% of the time, Pallas kernels for 0%

commit v1 on v0

v1 whole, which is shorter than its diff:
```python
import functools

import jax
import jax.numpy as jnp
from jax import lax
from jax.experimental import pallas as pl
from jax.experimental.pallas import tpu as pltpu
from jax.sharding import PartitionSpec as P

GROUP = 4
SUB = 16
WINDOW = 2
F32, BF16 = jnp.float32, jnp.bfloat16


def dot(a, b):
    return jnp.dot(a, b, preferred_element_type=F32)


def iota(shape, dim):
    return lax.broadcasted_iota(jnp.int32, shape, dim)


def layer_kernel(
    devices,
    cap,
    tokens_ref,
    routing_ref,
    gates_ref,
    gain_ref,
    wg_hbm,
    wu_hbm,
    wd_hbm,
    out_ref,
    wg,
    wu,
    wd,
    normed,
    target,
    weight,
    outgoing,
    mine,
    theirs,
    rows,
    hidden,
    kept,
    given,
    part,
    final,
    returned,
    w_sem,
    w_send,
    w_recv,
    d_send,
    d_recv,
    l_send,
    l_recv,
    p_send,
    p_recv,
    r_send,
    r_recv,
):
    tok, width = tokens_ref.shape
    ff = wg_hbm.shape[2]
    extra = cap - SUB
    folds = SUB // extra
    part_w = width // folds
    experts = devices // GROUP
    steps = experts // 2

    me = lax.axis_index("ep")
    core = me % 2
    pair = me // GROUP
    role = me // 2 % 2
    mate = me + 2 - 4 * role
    twin = me + 1 - 2 * core

    def device_of(pair_at, role_at):
        return lax.rem(pair_at + 2 * experts, experts) * GROUP + role_at * 2 + core

    def delta_of(step):
        return lax.rem(steps - step, steps)

    barrier = pltpu.get_barrier_semaphore()

    def greet(i, carry):
        pl.semaphore_signal(barrier, inc=1, device_id={"ep": lax.rem(me + 2 * i, devices)})
        return carry

    lax.fori_loop(1, devices // 2, greet, 0)
    pl.semaphore_signal(barrier, inc=1, device_id={"ep": twin})

    own_rows = pl.ds(pl.multiple_of(core * ff, 128), ff)
    own_weights = [
        (wg_hbm.at[0], wg.at[core]),
        (wu_hbm.at[0], wu.at[core]),
        (wd_hbm.at[0], wd.at[own_rows]),
    ]
    local_w = [
        pltpu.make_async_copy(src, dst, w_sem.at[i]) for i, (src, dst) in enumerate(own_weights)
    ]
    remote_w = [
        pltpu.make_async_remote_copy(
            src, dst, w_send.at[i], w_recv.at[i], device_id={"ep": twin}
        )
        for i, (src, dst) in enumerate(own_weights)
    ]
    for copy in local_w:
        copy.start()

    values = tokens_ref[...].astype(F32)
    scale = lax.rsqrt(jnp.mean(values * values, axis=-1, keepdims=True) + 1e-06)
    normed[...] = (values * scale * gain_ref[...].astype(F32)).astype(BF16)

    lane = iota((tok, tok), 1)
    named = [
        jnp.where(lane == routing_ref[:, k : k + 1], 1.0, 0.0).astype(F32) for k in range(2)
    ]
    earlier = jnp.where(lane < iota((tok, tok), 0), 1.0, 0.0).astype(BF16)
    before = dot(earlier, (named[0] + named[1]).astype(BF16))
    places = jnp.zeros((tok, tok), F32)
    for k in range(2):
        slot = jnp.sum(named[k] * before, axis=-1, keepdims=True)
        place = routing_ref[:, k : k + 1].astype(F32) * cap + slot
        places = jnp.where(lane == k, place, places)
        weight[:, k : k + 1] = place
    target[...] = places.T

    def block_of(expert):
        row = iota((2 * SUB, tok), 0)
        slot = jnp.where(row < SUB, row, SUB + row % extra)
        wanted = (expert * cap + slot).astype(F32)
        pick = jnp.where(target[0:1, :] == wanted, 1.0, 0.0) + jnp.where(
            target[1:2, :] == wanted, 1.0, 0.0
        )
        return dot(pick.astype(BF16), normed[...])

    def put_block(picked, ref):
        at = iota((SUB, part_w), 0) // extra
        folded = jnp.zeros((SUB, part_w), F32)
        for q in range(folds):
            columns = slice(q * part_w, (q + 1) * part_w)
            ref[q * SUB : (q + 1) * SUB, :] = picked[:SUB, columns].astype(BF16)
            folded = jnp.where(at == q, picked[SUB:, columns], folded)
        ref[folds * SUB :, :] = folded.astype(BF16)

    def send_to(expert, role_at, slot_step, slot_side):
        return pltpu.make_async_remote_copy(
            outgoing.at[expert],
            mine.at[slot_step, slot_side],
            d_send.at[expert],
            d_recv.at[slot_step * 2 + slot_side],
            device_id={"ep": device_of(expert, role_at)},
        )

    def dispatch(step):
        delta = delta_of(step)

        @pl.when(delta == 0)
        def _():
            far = lax.rem(pair + steps, experts)
            put_block(block_of(far), outgoing.at[far])
            send_to(far, 1 - role, 0, 1).start()
            put_block(block_of(pair), mine.at[0, 0])

        @pl.when(delta != 0)
        def _():
            for role_at in range(2):
                expert = lax.rem(pair + (1 - 2 * role_at) * delta + experts, experts)
                put_block(block_of(expert), outgoing.at[expert])
                send_to(expert, role_at, delta, role).start()

    def wait_arrival(slot_step, slot_side):
        pltpu.make_async_remote_copy(
            outgoing.at[0],
            mine.at[slot_step, slot_side],
            d_send.at[0],
            d_recv.at[slot_step * 2 + slot_side],
            device_id={"ep": mate},
        ).wait_recv()

    def relay(delta):
        return pltpu.make_async_remote_copy(
            mine.at[delta],
            theirs.at[delta],
            l_send.at[delta],
            l_recv.at[delta],
            device_id={"ep": mate},
        )

    def give(delta):
        return pltpu.make_async_remote_copy(
            given.at[delta],
            part.at[delta],
            p_send.at[delta],
            p_recv.at[delta],
            device_id={"ep": mate},
        )

    def send_back(delta, side):
        source = pair + (2 * role - 1) * delta
        return pltpu.make_async_remote_copy(
            final.at[delta, side],
            returned.at[pair],
            r_send.at[delta * 2 + side],
            r_recv.at[pair],
            device_id={"ep": device_of(source, side)},
        )

    def send_back_far():
        return pltpu.make_async_remote_copy(
            final.at[0, 1],
            returned.at[pair],
            r_send.at[1],
            r_recv.at[pair],
            device_id={"ep": device_of(pair + steps, 1 - role)},
        )

    def compute(delta):
        blocks = [mine.at[delta, 0], mine.at[delta, 1], theirs.at[delta, 0], theirs.at[delta, 1]]
        count = len(blocks)
        for b, block in enumerate(blocks):
            for q in range(folds):
                rows[b * SUB : (b + 1) * SUB, q * part_w : (q + 1) * part_w] = block[
                    q * SUB : (q + 1) * SUB, :
                ]
        folded = jnp.concatenate([block[folds * SUB :, :] for block in blocks], axis=0)
        main = count * SUB
        to = iota((count * extra, main), 0)
        at = iota((count * extra, main), 1)
        for q in range(folds):
            source = to // extra * SUB + q * extra + to % extra
            unfold = jnp.where(at == source, 1.0, 0.0).astype(BF16)
            rows[main:, q * part_w : (q + 1) * part_w] = dot(unfold, folded).astype(BF16)

        def half(h, carry):
            gate = dot(rows[...], wg[h])
            up = dot(rows[...], wu[h])
            hidden[h] = (jax.nn.silu(gate) * up).astype(BF16)
            return carry

        lax.fori_loop(0, 2, half, 0)
        to = iota((main, count * extra), 0)
        at = iota((main, count * extra), 1)
        refolded = jnp.zeros((main, part_w), F32)
        for q in range(folds):
            columns = slice(q * part_w, (q + 1) * part_w)
            piece = dot(hidden[0], wd[:ff, columns]) + dot(hidden[1], wd[ff:, columns])
            for b in range(2):
                kept[delta, b, q * SUB : (q + 1) * SUB, :] = piece[b * SUB : (b + 1) * SUB]
                given[delta, b, q * SUB : (q + 1) * SUB, :] = piece[
                    (b + 2) * SUB : (b + 3) * SUB
                ].astype(BF16)
            fold = (to // SUB == at // extra) & (to % SUB == q * extra + at % extra)
            refolded += dot(jnp.where(fold, 1.0, 0.0).astype(BF16), piece[main:].astype(BF16))
        for b in range(2):
            kept[delta, b, folds * SUB :, :] = refolded[b * SUB : (b + 1) * SUB]
            given[delta, b, folds * SUB :, :] = refolded[(b + 2) * SUB : (b + 3) * SUB].astype(BF16)

    pl.semaphore_wait(barrier, devices // 2)
    for step in range(WINDOW):
        dispatch(step)
    for copy in remote_w:
        copy.start()

    def body(step, carry):
        @pl.when(step < steps)
        def _():
            delta = delta_of(step)

            @pl.when(delta != 0)
            def _():
                wait_arrival(delta, 0)

            wait_arrival(delta, 1)
            relay(delta).start()

        @pl.when(step + WINDOW < steps)
        def _():
            dispatch(step + WINDOW)

        @pl.when((step >= 1) & (step <= steps))
        def _():
            delta = delta_of(step - 1)

            @pl.when(step == 1)
            def _():
                for copy in local_w:
                    copy.wait()
                for copy in remote_w:
                    copy.wait_recv()

            relay(delta).wait_recv()
            compute(delta)
            give(delta).start()

        @pl.when(step >= 2)
        def _():
            delta = delta_of(step - 2)
            give(delta).wait_recv()

            @pl.when(delta != 0)
            def _():
                final[delta] = (kept[delta] + part[delta].astype(F32)).astype(BF16)
                for side in range(2):
                    send_back(delta, side).start()

            @pl.when(delta == 0)
            def _():
                final[0, 1] = (kept[0, 1] + part[0, 1].astype(F32)).astype(BF16)
                send_back_far().start()
                returned[pair] = (kept[0, 0] + part[0, 0].astype(F32)).astype(BF16)

        return carry

    lax.fori_loop(0, steps + 2, body, 0)

    def wait_return(i, carry):
        expert = lax.rem(pair + i, experts)
        pltpu.make_async_remote_copy(
            final.at[0, 1],
            returned.at[expert],
            r_send.at[0],
            r_recv.at[expert],
            device_id={"ep": mate},
        ).wait_recv()
        return carry

    lax.fori_loop(1, experts, wait_return, 0)

    main = experts * SUB
    column = iota((tok, main), 1)
    wanted = (column // SUB * cap + column % SUB).astype(F32)
    wanted_extra = (column // SUB * cap + SUB + column % extra).astype(F32)
    share = jnp.zeros((tok, main), F32)
    share_extra = jnp.zeros((tok, main), F32)
    for k in range(2):
        place, gate = weight[:, k : k + 1], gates_ref[:, k : k + 1]
        share = jnp.where(place == wanted, gate, share)
        share_extra = jnp.where(place == wanted_extra, gate, share_extra)

    def split(value):
        high = value.astype(BF16)
        return high, (value - high.astype(F32)).astype(BF16)

    high, low = split(share)
    folded = returned[:, folds * SUB :, :].reshape(main, part_w)
    for q in range(folds):
        mask = column % SUB // extra == q
        high_extra, low_extra = split(jnp.where(mask, share_extra, 0.0))
        straight = returned[:, q * SUB : (q + 1) * SUB, :].reshape(main, part_w)
        mixed = dot(high, straight) + dot(low, straight)
        mixed += dot(high_extra, folded) + dot(low_extra, folded)
        out_ref[:, q * part_w : (q + 1) * part_w] = mixed.astype(BF16)

    for copy in remote_w:
        copy.wait_send()

    def drain(delta, carry):
        relay(delta).wait_send()
        give(delta).wait_send()

        @pl.when(delta != 0)
        def _():
            for side in range(2):
                send_back(delta, side).wait_send()

        @pl.when(delta == 0)
        def _():
            send_back_far().wait_send()

        return carry

    lax.fori_loop(0, steps, drain, 0)

    def drain_dispatch(i, carry):
        expert = lax.rem(pair + i, experts)
        send_to(expert, 0, 0, 1).wait_send()
        return carry

    lax.fori_loop(1, experts, drain_dispatch, 0)


def per_device(tokens, routing, gates, norm_gain, w_gate, w_up, w_down):
    tok, width = tokens.shape
    top = routing.shape[1]
    ff = w_gate.shape[2]
    devices = lax.axis_size("ep")
    experts = devices // GROUP
    steps = experts // 2
    cap = GROUP * (5 * tok * top // (4 * devices))
    extra = cap - SUB
    folds = SUB // extra
    assert top == 2 and 0 < extra and folds * extra == SUB and width % (folds * 128) == 0
    block = ((folds + 1) * SUB, width // folds)
    batch = 4 * cap
    pairs = (steps, 2) + block
    dma = pltpu.SemaphoreType.DMA
    vmem = pl.BlockSpec(memory_space=pltpu.VMEM)
    hbm = pl.BlockSpec(memory_space=pl.ANY)
    return pl.pallas_call(
        functools.partial(layer_kernel, devices, cap),
        out_shape=jax.ShapeDtypeStruct((tok, width), BF16),
        in_specs=[vmem, vmem, vmem, vmem, hbm, hbm, hbm],
        out_specs=vmem,
        scratch_shapes=[
            pltpu.VMEM((2, width, ff), BF16),
            pltpu.VMEM((2, width, ff), BF16),
            pltpu.VMEM((2 * ff, width), BF16),
            pltpu.VMEM((tok, width), BF16),
            pltpu.VMEM((tok, tok), F32),
            pltpu.VMEM((tok, 128), F32),
            pltpu.VMEM((experts,) + block, BF16),
            pltpu.VMEM(pairs, BF16),
            pltpu.VMEM(pairs, BF16),
            pltpu.VMEM((batch, width), BF16),
            pltpu.VMEM((2, batch, ff), BF16),
            pltpu.VMEM(pairs, F32),
            pltpu.VMEM(pairs, BF16),
            pltpu.VMEM(pairs, BF16),
            pltpu.VMEM(pairs, BF16),
            pltpu.VMEM((experts,) + block, BF16),
            dma((3,)),
            dma((3,)),
            dma((3,)),
            dma((experts,)),
            dma((experts,)),
            dma((steps,)),
            dma((steps,)),
            dma((steps,)),
            dma((steps,)),
            dma((experts,)),
            dma((experts,)),
        ],
        compiler_params=pltpu.CompilerParams(
            collective_id=0, has_side_effects=True, vmem_limit_bytes=60 * 1024 * 1024
        ),
    )(tokens, routing, gates, norm_gain.reshape(1, width), w_gate, w_up, w_down)


def solution(mesh):
    placed = (
        P(("grp", "ep"), None),
        P(("grp", "ep"), None),
        P(("grp", "ep"), None),
        P(),
        P("ep", None, None),
        P("ep", None, None),
        P("ep", None, None),
    )
    return jax.shard_map(
        per_device, mesh=mesh, in_specs=placed, out_specs=P(("grp", "ep"), None), check_vma=False
    )
```

time: 639 us -> 304 us (0.48)
  Pallas kernels: 0 us -> 298 us
  waiting for transfers between devices: 296 us -> 0 us
  blocking collectives: 233 us -> 0 us
  local copies, waits for them, and re-layouts: 44 us -> 5.98 us
  other arithmetic: 32.9 us -> 0 us
  matrix products: 23.6 us -> 0 us
  starting transfers between devices: 7.7 us -> 0 us
    pallas_call x0 -> x1, Pallas kernels: none -> 298 us  [per_device(): pl.pallas_call(functools.partial(layer_kernel, devices, cap), out_shape=j...]
    all_to_all x1 -> x0, blocking collectives: 233 us -> none  [per_device(): lax.all_to_all(outgoing.reshape(devices, member_slots, model_width), 'ep'...]
    all_to_all x1 -> x0, waiting for transfers between devices: 199 us -> none  [per_device(): lax.all_to_all(finished, 'ep', split_axis=0, concat_axis=0, tiled=True)]
    ppermute x4 -> x0, waiting for transfers between devices: 97.7 us -> none  [partner_2(): lax.ppermute(x, axis, [(i, i ^ 1 << distance) for i in range(lax.axis_siz...]
    dot_general x3 -> x0, matrix products: 23.6 us -> none  [the longest x1 8.88 us: per_device(): jnp.dot(hidden, w_down[0], preferred_element_type=jnp.float32)]
    another operation x1 -> x0, local copies, waits for them, and re-layouts: 10 us -> none  [per_device(): expert_rows = arrived.reshape(devices * capacity, model_width)]
    concatenate x2 -> x0, local copies, waits for them, and re-layouts: 9.96 us -> none  [per_device(): pieces = jnp.concatenate([lower_half, upper_half], axis=1)]
    concatenate x2 -> x0, other arithmetic: 9.32 us -> none  [per_device(): pieces = jnp.concatenate([lower_half, upper_half], axis=1)]
  transfers between devices with their start and end apart: 5 -> 0, of which waited for: 5 -> 0; matrix products, arithmetic and copies ran while one was open for 0% -> 0% of each run, Pallas kernels for 0% -> 0%
where the time goes in v1:
time: 304 us
  Pallas kernels  298 us (98%)
  local copies, waits for them, and re-layouts  5.98 us (2%)
    pallas_call x1, Pallas kernels, per_device(): pl.pallas_call(functools.partial(layer_kernel, devices, cap), out_shape=j...  298 us

profile of v1, /device:TPU:44, one launch (start us, length us, event | category | flops | bytes accessed | tf_op | source)
XLA Modules:
  0.0 304.1 jit_solution(609670278704998157)
XLA Ops:
  0.0 1.3 reshape.3.gain_ref
  1.3 1.4 copy.8.routing_ref
  2.7 1.4 copy.9.gates_ref
  4.1 298.1 %shard_map.73 = bf16[128,2048]{1,0:T(8,128)(2,1)} custom-call(bf16[128,2048]{1,0:T(8,128)(2,1)} %tokens_ref.1, s32[128,2]{1,0:T(8,128)} %copy.8.routing_ref, f32[128,2]{1,0:T(8,128)} %copy.9.gates_ref, bf16[1,2048]{1,0:T(2,128)(2,1)} %reshape.3.gain_ref, bf16[1,2048,896]{2,1,0:T(8,128)(2,1)} %wg_hbm.1, bf16[1,2048,896]{2,1,0:T(8,128)(2,1)} %wu_hbm.1, ...), custom_call_target="tpu_custom_call" | custom-call | tf_op jit(solution)/shard_map/pallas_call | solution.py:401
  302.2 1.9 copy.11

commit v2 on v1

--- a/solution.py
+++ b/solution.py
@@ -8,8 +8,8 @@
 from jax.sharding import PartitionSpec as P
 
 GROUP = 4
+LANES = 128
 SUB = 16
-WINDOW = 2
 F32, BF16 = jnp.float32, jnp.bfloat16
 
 
@@ -38,6 +38,7 @@
     normed,
     target,
     weight,
+    total,
     outgoing,
     mine,
     theirs,
@@ -79,7 +80,8 @@
         return lax.rem(pair_at + 2 * experts, experts) * GROUP + role_at * 2 + core
 
     def delta_of(step):
-        return lax.rem(steps - step, steps)
+        rising = lax.rem(2 * step + 2, steps)
+        return jnp.where(step < steps // 2, rising, 2 * (steps - step) - 1)
 
     barrier = pltpu.get_barrier_semaphore()
 
@@ -110,21 +112,21 @@
 
     values = tokens_ref[...].astype(F32)
     scale = lax.rsqrt(jnp.mean(values * values, axis=-1, keepdims=True) + 1e-06)
-    normed[...] = (values * scale * gain_ref[...].astype(F32)).astype(BF16)
-
-    lane = iota((tok, tok), 1)
+    for j in range(width // LANES):
+        columns = slice(j * LANES, (j + 1) * LANES)
+        gain = gain_ref[j : j + 1, :].astype(F32)
+        normed[:, columns] = (values[:, columns] * scale * gain).astype(BF16)
+
     named = [
-        jnp.where(lane == routing_ref[:, k : k + 1], 1.0, 0.0).astype(F32) for k in range(2)
+        jnp.where(iota((experts, tok), 0) == routing_ref[k : k + 1, :], 1.0, 0.0).astype(F32)
+        for k in range(2)
     ]
-    earlier = jnp.where(lane < iota((tok, tok), 0), 1.0, 0.0).astype(BF16)
-    before = dot(earlier, (named[0] + named[1]).astype(BF16))
-    places = jnp.zeros((tok, tok), F32)
+    earlier = jnp.where(iota((tok, tok), 0) < iota((tok, tok), 1), 1.0, 0.0).astype(BF16)
+    before = dot((named[0] + named[1]).astype(BF16), earlier)
+    target[...] = jnp.zeros_like(target)
     for k in range(2):
-        slot = jnp.sum(named[k] * before, axis=-1, keepdims=True)
-        place = routing_ref[:, k : k + 1].astype(F32) * cap + slot
-        places = jnp.where(lane == k, place, places)
-        weight[:, k : k + 1] = place
-    target[...] = places.T
+        slot = jnp.sum(named[k] * before, axis=0, keepdims=True)
+        target[k : k + 1, :] = routing_ref[k : k + 1, :].astype(F32) * cap + slot
 
     def block_of(expert):
         row = iota((2 * SUB, tok), 0)
@@ -258,10 +260,18 @@
             given[delta, b, folds * SUB :, :] = refolded[(b + 2) * SUB : (b + 3) * SUB].astype(BF16)
 
     pl.semaphore_wait(barrier, devices // 2)
-    for step in range(WINDOW):
+
+    def dispatch_all(step, carry):
         dispatch(step)
-    for copy in remote_w:
-        copy.start()
+
+        @pl.when(step == 1)
+        def _():
+            for copy in remote_w:
+                copy.start()
+
+        return carry
+
+    lax.fori_loop(0, steps, dispatch_all, 0)
 
     def body(step, carry):
         @pl.when(step < steps)
@@ -274,10 +284,6 @@
 
             wait_arrival(delta, 1)
             relay(delta).start()
-
-        @pl.when(step + WINDOW < steps)
-        def _():
-            dispatch(step + WINDOW)
 
         @pl.when((step >= 1) & (step <= steps))
         def _():
@@ -315,8 +321,11 @@
 
     lax.fori_loop(0, steps + 2, body, 0)
 
-    def wait_return(i, carry):
-        expert = lax.rem(pair + i, experts)
+    target[2:4, :] = gates_ref[...]
+    weight[...] = target[...].T
+    total[...] = jnp.zeros_like(total)
+
+    def wait_return(expert):
         pltpu.make_async_remote_copy(
             final.at[0, 1],
             returned.at[expert],
@@ -324,34 +333,60 @@
             r_recv.at[expert],
             device_id={"ep": mate},
         ).wait_recv()
-        return carry
-
-    lax.fori_loop(1, experts, wait_return, 0)
-
-    main = experts * SUB
-    column = iota((tok, main), 1)
-    wanted = (column // SUB * cap + column % SUB).astype(F32)
-    wanted_extra = (column // SUB * cap + SUB + column % extra).astype(F32)
-    share = jnp.zeros((tok, main), F32)
-    share_extra = jnp.zeros((tok, main), F32)
-    for k in range(2):
-        place, gate = weight[:, k : k + 1], gates_ref[:, k : k + 1]
-        share = jnp.where(place == wanted, gate, share)
-        share_extra = jnp.where(place == wanted_extra, gate, share_extra)
 
     def split(value):
         high = value.astype(BF16)
-        return high, (value - high.astype(F32)).astype(BF16)
-
-    high, low = split(share)
-    folded = returned[:, folds * SUB :, :].reshape(main, part_w)
-    for q in range(folds):
-        mask = column % SUB // extra == q
-        high_extra, low_extra = split(jnp.where(mask, share_extra, 0.0))
-        straight = returned[:, q * SUB : (q + 1) * SUB, :].reshape(main, part_w)
-        mixed = dot(high, straight) + dot(low, straight)
-        mixed += dot(high_extra, folded) + dot(low_extra, folded)
-        out_ref[:, q * part_w : (q + 1) * part_w] = mixed.astype(BF16)
+        return [high, (value - high.astype(F32)).astype(BF16)]
+
+    def collect(i, carry):
+        near = [delta_of(2 * i), delta_of(2 * i + 1)]
+        group = []
+        for delta in near:
+            group.append(lax.rem(pair + jnp.where(delta == 0, steps, delta), experts))
+            group.append(lax.rem(pair - delta + experts, experts))
+        count = len(group) * SUB
+        column = iota((tok, count), 1)
+        row = column % SUB
+        first = jnp.zeros((tok, count), jnp.int32)
+        for j, expert in enumerate(group):
+            first = jnp.where(column // SUB == j, expert * cap, first)
+        straight = jnp.zeros((tok, count), F32)
+        folded = jnp.zeros((tok, count), F32)
+        for k in range(2):
+            place, gate = weight[:, k : k + 1], weight[:, k + 2 : k + 3]
+            straight = jnp.where(place == (first + row).astype(F32), gate, straight)
+            folded = jnp.where(place == (first + SUB + row % extra).astype(F32), gate, folded)
+        shares = jnp.concatenate(split(straight), axis=0)
+        shares_folded = []
+        for q in range(folds):
+            shares_folded += split(jnp.where(row // extra == q, folded, 0.0))
+        shares_folded = jnp.concatenate(shares_folded, axis=0)
+
+        for j, (delta, expert) in enumerate(zip([near[0], near[0], near[1], near[1]], group)):
+            if j % 2 == 0:
+                wait_return(expert)
+            else:
+
+                @pl.when(delta != 0)
+                def _():
+                    wait_return(expert)
+
+        def rows_of(q):
+            return jnp.concatenate(
+                [returned[expert, q * SUB : (q + 1) * SUB, :] for expert in group], axis=0
+            )
+
+        more = dot(shares_folded, rows_of(folds))
+        for q in range(folds):
+            some = dot(shares, rows_of(q))
+            part_sum = some[:tok] + some[tok:]
+            part_sum += more[2 * q * tok : (2 * q + 1) * tok]
+            part_sum += more[(2 * q + 1) * tok : (2 * q + 2) * tok]
+            total[:, q * part_w : (q + 1) * part_w] += part_sum
+        return carry
+
+    lax.fori_loop(0, steps // 2, collect, 0)
+    out_ref[...] = total[...].astype(BF16)
 
     for copy in remote_w:
         copy.wait_send()
@@ -391,7 +426,8 @@
     cap = GROUP * (5 * tok * top // (4 * devices))
     extra = cap - SUB
     folds = SUB // extra
-    assert top == 2 and 0 < extra and folds * extra == SUB and width % (folds * 128) == 0
+    assert top == 2 and tok == LANES and steps % 2 == 0
+    assert 0 < extra and folds * extra == SUB and width % (folds * LANES) == 0
     block = ((folds + 1) * SUB, width // folds)
     batch = 4 * cap
     pairs = (steps, 2) + block
@@ -409,7 +445,8 @@
             pltpu.VMEM((2 * ff, width), BF16),
             pltpu.VMEM((tok, width), BF16),
             pltpu.VMEM((tok, tok), F32),
-            pltpu.VMEM((tok, 128), F32),
+            pltpu.VMEM((tok, tok), F32),
+            pltpu.VMEM((tok, width), F32),
             pltpu.VMEM((experts,) + block, BF16),
             pltpu.VMEM(pairs, BF16),
             pltpu.VMEM(pairs, BF16),
@@ -435,7 +472,7 @@
         compiler_params=pltpu.CompilerParams(
             collective_id=0, has_side_effects=True, vmem_limit_bytes=60 * 1024 * 1024
         ),
-    )(tokens, routing, gates, norm_gain.reshape(1, width), w_gate, w_up, w_down)
+    )(tokens, routing.T, gates.T, norm_gain.reshape(width // LANES, LANES), w_gate, w_up, w_down)
 
 
 def solution(mesh):

time: 304 us -> 296 us (0.974)
  local copies, waits for them, and re-layouts: 5.98 us -> 1.88 us
  Pallas kernels: 298 us -> 294 us
    pallas_call x1, Pallas kernels: 298 us -> 294 us  [per_device(): pl.pallas_call(functools.partial(layer_kernel, devices, cap), out_shape=j...]
where the time goes in v2:
time: 296 us
  Pallas kernels  294 us (99%)
    pallas_call x1, Pallas kernels, per_device(): pl.pallas_call(functools.partial(layer_kernel, devices, cap), out_shape=j...  294 us

profile of v2, /device:TPU:44, one launch (start us, length us, event | category | flops | bytes accessed | tf_op | source)
XLA Modules:
  0.0 295.6 jit_solution(5450602766577231462)
XLA Ops:
  0.0 293.7 %shard_map.73 = bf16[128,2048]{1,0:T(8,128)(2,1)} custom-call(bf16[128,2048]{1,0:T(8,128)(2,1)} %tokens_ref.1, s32[2,128]{1,0:T(2,128)} %bitcast.4, f32[2,128]{1,0:T(2,128)} %bitcast.5, bf16[16,128]{1,0:T(8,128)(2,1)} %bitcast.3, bf16[1,2048,896]{2,1,0:T(8,128)(2,1)} %wg_hbm.1, bf16[1,2048,896]{2,1,0:T(8,128)(2,1)} %wu_hbm.1, bf16[1,896,2048]{2,1,0:T(8,128)(2,1)} %wd_hbm.1), custom_call_target="tpu_custom_call" | custom-call | tf_op jit(solution)/shard_map/pallas_call | solution.py:437
  293.7 1.9 copy.9

commit v3 on v2

--- a/solution.py
+++ b/solution.py
@@ -9,6 +9,7 @@
 
 GROUP = 4
 LANES = 128
+WINDOW = 4
 SUB = 16
 F32, BF16 = jnp.float32, jnp.bfloat16
 
@@ -24,7 +25,7 @@
 def layer_kernel(
     devices,
     cap,
-    tokens_ref,
+    tokens_hbm,
     routing_ref,
     gates_ref,
     gain_ref,
@@ -35,6 +36,7 @@
     wg,
     wu,
     wd,
+    tokens_ref,
     normed,
     target,
     weight,
@@ -49,6 +51,9 @@
     part,
     final,
     returned,
+    up,
+    down,
+    t_sem,
     w_sem,
     w_send,
     w_recv,
@@ -61,7 +66,7 @@
     r_send,
     r_recv,
 ):
-    tok, width = tokens_ref.shape
+    tok, width = tokens_hbm.shape
     ff = wg_hbm.shape[2]
     extra = cap - SUB
     folds = SUB // extra
@@ -83,15 +88,28 @@
         rising = lax.rem(2 * step + 2, steps)
         return jnp.where(step < steps // 2, rising, 2 * (steps - step) - 1)
 
+    below, above = lax.rem(me + devices - 2, devices), lax.rem(me + 2, devices)
+    reach = devices // 4 - 1
     barrier = pltpu.get_barrier_semaphore()
-
-    def greet(i, carry):
-        pl.semaphore_signal(barrier, inc=1, device_id={"ep": lax.rem(me + 2 * i, devices)})
+    for other in (below, above, twin):
+        pl.semaphore_signal(barrier, inc=1, device_id={"ep": other})
+
+    def pass_on(k):
+        pl.semaphore_signal(up.at[k], inc=1, device_id={"ep": below})
+        pl.semaphore_signal(down.at[k], inc=1, device_id={"ep": above})
+
+    def learn(k, carry):
+        pl.semaphore_wait(up.at[k], 1)
+        pl.semaphore_wait(down.at[k], 1)
+
+        @pl.when(k + 1 < reach)
+        def _():
+            pass_on(k + 1)
+
         return carry
 
-    lax.fori_loop(1, devices // 2, greet, 0)
-    pl.semaphore_signal(barrier, inc=1, device_id={"ep": twin})
-
+    fetch = pltpu.make_async_copy(tokens_hbm, tokens_ref, t_sem)
+    fetch.start()
     own_rows = pl.ds(pl.multiple_of(core * ff, 128), ff)
     own_weights = [
         (wg_hbm.at[0], wg.at[core]),
@@ -110,13 +128,6 @@
     for copy in local_w:
         copy.start()
 
-    values = tokens_ref[...].astype(F32)
-    scale = lax.rsqrt(jnp.mean(values * values, axis=-1, keepdims=True) + 1e-06)
-    for j in range(width // LANES):
-        columns = slice(j * LANES, (j + 1) * LANES)
-        gain = gain_ref[j : j + 1, :].astype(F32)
-        normed[:, columns] = (values[:, columns] * scale * gain).astype(BF16)
-
     named = [
         jnp.where(iota((experts, tok), 0) == routing_ref[k : k + 1, :], 1.0, 0.0).astype(F32)
         for k in range(2)
@@ -128,6 +139,14 @@
         slot = jnp.sum(named[k] * before, axis=0, keepdims=True)
         target[k : k + 1, :] = routing_ref[k : k + 1, :].astype(F32) * cap + slot
 
+    fetch.wait()
+    values = tokens_ref[...].astype(F32)
+    scale = lax.rsqrt(jnp.mean(values * values, axis=-1, keepdims=True) + 1e-06)
+    for j in range(width // LANES):
+        columns = slice(j * LANES, (j + 1) * LANES)
+        gain = gain_ref[j : j + 1, :].astype(F32)
+        normed[:, columns] = (values[:, columns] * scale * gain).astype(BF16)
+
     def block_of(expert):
         row = iota((2 * SUB, tok), 0)
         slot = jnp.where(row < SUB, row, SUB + row % extra)
@@ -157,6 +176,9 @@
 
     def dispatch(step):
         delta = delta_of(step)
+        known = jnp.maximum(4 * step, 1)
+        wanted = jnp.where(step < steps // 2, jnp.minimum(4 * step + 4, reach), known)
+        lax.fori_loop(known, wanted, learn, 0)
 
         @pl.when(delta == 0)
         def _():
@@ -181,12 +203,12 @@
             device_id={"ep": mate},
         ).wait_recv()
 
-    def relay(delta):
+    def relay(delta, side):
         return pltpu.make_async_remote_copy(
-            mine.at[delta],
-            theirs.at[delta],
-            l_send.at[delta],
-            l_recv.at[delta],
+            mine.at[delta, side],
+            theirs.at[delta, side],
+            l_send.at[2 * delta + side],
+            l_recv.at[2 * delta + side],
             device_id={"ep": mate},
         )
 
@@ -259,19 +281,11 @@
             kept[delta, b, folds * SUB :, :] = refolded[b * SUB : (b + 1) * SUB]
             given[delta, b, folds * SUB :, :] = refolded[(b + 2) * SUB : (b + 3) * SUB].astype(BF16)
 
-    pl.semaphore_wait(barrier, devices // 2)
-
-    def dispatch_all(step, carry):
-        dispatch(step)
-
-        @pl.when(step == 1)
-        def _():
-            for copy in remote_w:
-                copy.start()
-
-        return carry
-
-    lax.fori_loop(0, steps, dispatch_all, 0)
+    pl.semaphore_wait(barrier, 3)
+    pass_on(1)
+    lax.fori_loop(0, WINDOW, lambda step, carry: (dispatch(step), carry)[1], 0)
+    for copy in remote_w:
+        copy.start()
 
     def body(step, carry):
         @pl.when(step < steps)
@@ -282,8 +296,13 @@
             def _():
                 wait_arrival(delta, 0)
 
+            relay(delta, 0).start()
             wait_arrival(delta, 1)
-            relay(delta).start()
+            relay(delta, 1).start()
+
+        @pl.when(step + WINDOW < steps)
+        def _():
+            dispatch(step + WINDOW)
 
         @pl.when((step >= 1) & (step <= steps))
         def _():
@@ -296,7 +315,8 @@
                 for copy in remote_w:
                     copy.wait_recv()
 
-            relay(delta).wait_recv()
+            for side in range(2):
+                relay(delta, side).wait_recv()
             compute(delta)
             give(delta).start()
 
@@ -392,7 +412,8 @@
         copy.wait_send()
 
     def drain(delta, carry):
-        relay(delta).wait_send()
+        for side in range(2):
+            relay(delta, side).wait_send()
         give(delta).wait_send()
 
         @pl.when(delta != 0)
@@ -433,16 +454,17 @@
     pairs = (steps, 2) + block
     dma = pltpu.SemaphoreType.DMA
     vmem = pl.BlockSpec(memory_space=pltpu.VMEM)
-    hbm = pl.BlockSpec(memory_space=pl.ANY)
+    hbm = pl.BlockSpec(memory_space=pltpu.HBM)
     return pl.pallas_call(
         functools.partial(layer_kernel, devices, cap),
         out_shape=jax.ShapeDtypeStruct((tok, width), BF16),
-        in_specs=[vmem, vmem, vmem, vmem, hbm, hbm, hbm],
+        in_specs=[hbm, vmem, vmem, vmem, hbm, hbm, hbm],
         out_specs=vmem,
         scratch_shapes=[
             pltpu.VMEM((2, width, ff), BF16),
             pltpu.VMEM((2, width, ff), BF16),
             pltpu.VMEM((2 * ff, width), BF16),
+            pltpu.VMEM((tok, width), BF16),
             pltpu.VMEM((tok, width), BF16),
             pltpu.VMEM((tok, tok), F32),
             pltpu.VMEM((tok, tok), F32),
@@ -457,13 +479,16 @@
             pltpu.VMEM(pairs, BF16),
             pltpu.VMEM(pairs, BF16),
             pltpu.VMEM((experts,) + block, BF16),
+            pltpu.SemaphoreType.REGULAR((devices // 4,)),
+            pltpu.SemaphoreType.REGULAR((devices // 4,)),
+            dma,
             dma((3,)),
             dma((3,)),
             dma((3,)),
             dma((experts,)),
             dma((experts,)),
-            dma((steps,)),
-            dma((steps,)),
+            dma((experts,)),
+            dma((experts,)),
             dma((steps,)),
             dma((steps,)),
             dma((experts,)),

time: 296 us -> 296 us (level)
  no operation moved by 1% of the time
where the time goes in v3:
time: 296 us; the launch traced here: 294 us
  Pallas kernels  292 us (99%)
    pallas_call x1, Pallas kernels, per_device(): pl.pallas_call(functools.partial(layer_kernel, devices, cap), out_shape=j...  292 us

profile of v3, /device:TPU:44, one launch (start us, length us, event | category | flops | bytes accessed | tf_op | source)
XLA Modules:
  0.0 294.3 jit_solution(243072906018706677)
XLA Ops:
  0.0 292.4 %shard_map.73 = bf16[128,2048]{1,0:T(8,128)(2,1)} custom-call(bf16[128,2048]{1,0:T(8,128)(2,1)} %tokens_hbm.1, s32[2,128]{1,0:T(2,128)} %bitcast.4, f32[2,128]{1,0:T(2,128)} %bitcast.5, bf16[16,128]{1,0:T(8,128)(2,1)} %bitcast.3, bf16[1,2048,896]{2,1,0:T(8,128)(2,1)} %wg_hbm.1, bf16[1,2048,896]{2,1,0:T(8,128)(2,1)} %wu_hbm.1, bf16[1,896,2048]{2,1,0:T(8,128)(2,1)} %wd_hbm.1), custom_call_target="tpu_custom_call" | custom-call | tf_op jit(solution)/shard_map/pallas_call | solution.py:458
  292.4 1.9 copy.9

commit v4 on v3

--- a/solution.py
+++ b/solution.py
@@ -9,7 +9,7 @@
 
 GROUP = 4
 LANES = 128
-WINDOW = 4
+WINDOW = 8
 SUB = 16
 F32, BF16 = jnp.float32, jnp.bfloat16
 

time: 296 us -> 297 us (level)
  no operation moved by 1% of the time
where the time goes in v4:
time: 297 us; the launch traced here: 295 us
  Pallas kernels  293 us (99%)
    pallas_call x1, Pallas kernels, per_device(): pl.pallas_call(functools.partial(layer_kernel, devices, cap), out_shape=j...  293 us

profile of v4, /device:TPU:44, one launch (start us, length us, event | category | flops | bytes accessed | tf_op | source)
XLA Modules:
  0.0 295.1 jit_solution(7780192336436753508)
XLA Ops:
  0.0 293.2 %shard_map.73 = bf16[128,2048]{1,0:T(8,128)(2,1)} custom-call(bf16[128,2048]{1,0:T(8,128)(2,1)} %tokens_hbm.1, s32[2,128]{1,0:T(2,128)} %bitcast.4, f32[2,128]{1,0:T(2,128)} %bitcast.5, bf16[16,128]{1,0:T(8,128)(2,1)} %bitcast.3, bf16[1,2048,896]{2,1,0:T(8,128)(2,1)} %wg_hbm.1, bf16[1,2048,896]{2,1,0:T(8,128)(2,1)} %wu_hbm.1, bf16[1,896,2048]{2,1,0:T(8,128)(2,1)} %wd_hbm.1), custom_call_target="tpu_custom_call" | custom-call | tf_op jit(solution)/shard_map/pallas_call | solution.py:458
  293.3 1.9 copy.9
